TPU v7x, 128 devices: a whole 4x4x4 slice. The times are simulated.
128 devices in a mesh: sp: 16 (over z, x), dp: 8 (over y, core).
Axes of the slice: x: 4, y: 4, z: 4, core: 2. Of those that a mesh axis runs over, the one named last changes fastest.
Arguments:
- residual_in: bfloat16 [8, 2048, 2048], P('dp', 'sp'), may hold values from -6 to 6
- query_rows: bfloat16 [8, 2048, 1024], P('dp', 'sp'), may hold values from -40 to 40
- key_rows: bfloat16 [8, 2048, 1024], P('dp', 'sp'), may hold values from -40 to 40
- value_rows: bfloat16 [8, 2048, 1024], P('dp', 'sp'), may hold values from -6 to 6
- gate_sums: float32 [8, 16, 2048], P('dp', 'sp'), as said below
- out_weight: bfloat16 [1024, 2048], replicated, may hold values from -0.1875 to 0.1875
- mix_gain: float32 [2048], replicated, may hold values from 0.1 to 1.9
- ffn_gain: float32 [2048], replicated, may hold values from 0.1 to 1.9
- expert_ids: int32 [8, 2048, 4], P('dp', 'sp'), may hold values from 0 to 127, all different within a row; in each aligned block of 128 rows (0 to 127, 128 to 255, ..., all dimensions but the last counted through in order) at most 8 rows name the same one
- route_weights: float32 [8, 2048, 4], P('dp', 'sp'), may hold values from 0.3 to 2
- expert_gate: bfloat16 [128, 2048, 512], P(('sp', 'dp')), may hold values from -0.125 to 0.125
- expert_up: bfloat16 [128, 2048, 512], P(('sp', 'dp')), may hold values from -0.125 to 0.125
- expert_down: bfloat16 [128, 512, 2048], P(('sp', 'dp')), may hold values from -0.25 to 0.25
- shared_gate: bfloat16 [2048, 512], replicated, may hold values from -0.125 to 0.125
- shared_up: bfloat16 [2048, 512], replicated, may hold values from -0.125 to 0.125
- shared_down: bfloat16 [512, 2048], replicated, may hold values from -0.25 to 0.25
Outputs:
- result_rows: bfloat16 [8, 2048, 2048], P('dp', 'sp')
Inputs may be any that keep to these rules, and one draw needn't show every extreme that they name: `expert_ids`: each row names 4 different experts. In the rows of one device no expert is named more than 8 times, a bound that some block reaches in some devices' rows. `gate_sums`: Non-increasing along positions for every sequence and head.
All inputs are finite; a program needn't handle non-finite values.
Results may differ from a plain program's by a relative error of at most 0.0071.
Values may be sent and summed in bfloat16 or wider, within the bound.
A program may use at most 128 MiB of HBM per device.

v0:
```python
import jax
import jax.numpy as jnp
from jax import lax
from jax.sharding import PartitionSpec as P

HEAD_DIM = 64


def sent_together(arrays, axis, split_dim, concat_dim, along):
    both = jnp.concatenate(arrays, axis=along)
    out, at, gathered = (
        lax.all_to_all(both, axis, split_axis=split_dim, concat_axis=concat_dim, tiled=True),
        0,
        [],
    )
    for a in arrays:
        gathered.append(lax.slice_in_dim(out, at, at + a.shape[along], axis=along))
        at += a.shape[along]
    return tuple(gathered)


def attend(query_all, key_all, value_all, gate_sums):
    length = query_all.shape[1]
    head_count = gate_sums.shape[1]
    score_scale = HEAD_DIM ** (-0.5)
    query_heads = query_all[0].reshape(length, head_count, HEAD_DIM)
    key_heads = key_all[0].reshape(length, head_count, HEAD_DIM)
    value_heads = value_all[0].reshape(length, head_count, HEAD_DIM)
    sums_local = gate_sums[0]
    block_rows = min(512, length)
    pieces = []
    for block_index in range(length // block_rows):
        start = block_index * block_rows
        block_end = start + block_rows
        scores = (
            jnp.einsum(
                "qhd,khd->hqk",
                query_heads[start:block_end],
                key_heads[:block_end],
                preferred_element_type=jnp.float32,
            )
            * score_scale
        )
        scores = scores + sums_local[:, start:block_end, None] - sums_local[:, None, :block_end]
        causal_mask = jnp.arange(block_end)[None, :] <= jnp.arange(start, block_end)[:, None]
        scores = jnp.where(causal_mask[None], scores, -jnp.inf)
        peak = jnp.max(scores, axis=2, keepdims=True)
        weights = jnp.exp(scores - peak)
        weights = (weights / jnp.sum(weights, axis=2, keepdims=True)).astype(jnp.bfloat16)
        mixed_heads = jnp.einsum(
            "hqk,khd->qhd", weights, value_heads[:block_end], preferred_element_type=jnp.float32
        ).astype(jnp.bfloat16)
        pieces.append(mixed_heads.reshape(block_rows, head_count * HEAD_DIM))
    return jnp.concatenate(pieces, axis=0)[None]


def gated_rows(rows_in, gate_w, up_w):
    gate_rows = jnp.dot(rows_in, gate_w, preferred_element_type=jnp.float32)
    up_rows = jnp.dot(rows_in, up_w, preferred_element_type=jnp.float32)
    return (jax.nn.silu(gate_rows) * up_rows).astype(jnp.bfloat16)


def shards(
    residual_in,
    query_rows,
    key_rows,
    value_rows,
    gate_sums,
    out_weight,
    mix_gain,
    ffn_gain,
    expert_ids,
    route_weights,
    expert_gate,
    expert_up,
    expert_down,
    shared_gate,
    shared_up,
    shared_down,
):
    key_all, value_all = sent_together((key_rows, value_rows), "sp", 2, 1, 0)
    query_all = lax.all_to_all(query_rows, "sp", split_axis=2, concat_axis=1, tiled=True)
    attended = attend(query_all, key_all, value_all, gate_sums)
    returned = lax.all_to_all(attended, "sp", split_axis=1, concat_axis=2, tiled=True)
    projected = jnp.dot(returned[0], out_weight, preferred_element_type=jnp.float32)
    residual_f = residual_in[0].astype(jnp.float32)
    mixed_rows = residual_f + mix_gain * projected * lax.rsqrt(
        jnp.mean(projected * projected, axis=1, keepdims=True) + 1e-06
    )
    normed = (
        ffn_gain
        * mixed_rows
        * lax.rsqrt(jnp.mean(mixed_rows * mixed_rows, axis=1, keepdims=True) + 1e-06)
    ).astype(jnp.bfloat16)
    shared_hidden = gated_rows(normed, shared_gate, shared_up)
    shared_out = jnp.dot(shared_hidden, shared_down, preferred_element_type=jnp.float32)
    tok_count = residual_in.shape[1]
    top_count = expert_ids.shape[2]
    width = residual_in.shape[2]
    sp_count = lax.axis_size("sp")
    dp_count = lax.axis_size("dp")
    expert_count = sp_count * dp_count
    capacity = 2 * tok_count * top_count // expert_count
    expert_list = expert_ids[0].reshape(tok_count * top_count)
    one_hot = (expert_list[:, None] == jnp.arange(expert_count, dtype=jnp.int32)[None, :]).astype(
        jnp.int32
    )
    position_in = jnp.sum((jnp.cumsum(one_hot, axis=0) - one_hot) * one_hot, axis=1)
    slot_index = expert_list * capacity + position_in
    repeated = jnp.repeat(normed, top_count, axis=0)
    outgoing = (
        jnp.zeros((expert_count * capacity, width), jnp.bfloat16).at[slot_index].set(repeated)
    )
    arrived = lax.all_to_all(
        outgoing.reshape(expert_count, capacity, width),
        ("sp", "dp"),
        split_axis=0,
        concat_axis=0,
        tiled=True,
    )
    flat_rows = arrived.reshape(-1, width)
    hidden = gated_rows(flat_rows, expert_gate[0], expert_up[0])
    finished = jnp.dot(hidden, expert_down[0], preferred_element_type=jnp.float32).astype(
        jnp.bfloat16
    )
    received = lax.all_to_all(
        finished.reshape(arrived.shape), ("sp", "dp"), split_axis=0, concat_axis=0, tiled=True
    )
    picked = received.reshape(expert_count * capacity, width)[slot_index]
    picked = picked.reshape(tok_count, top_count, width).astype(jnp.float32)
    routed = jnp.sum(picked * route_weights[0][:, :, None], axis=1)
    result_rows = (mixed_rows + shared_out + routed).astype(jnp.bfloat16)
    return result_rows[None]


def solution(mesh):
    return jax.shard_map(
        shards,
        mesh=mesh,
        in_specs=(
            P("dp", "sp", None),
            P("dp", "sp", None),
            P("dp", "sp", None),
            P("dp", "sp", None),
            P("dp", "sp", None),
            P(),
            P(),
            P(),
            P("dp", "sp", None),
            P("dp", "sp", None),
            P(("sp", "dp"), None, None),
            P(("sp", "dp"), None, None),
            P(("sp", "dp"), None, None),
            P(),
            P(),
            P(),
        ),
        out_specs=P("dp", "sp", None),
        check_vma=False,
    )
```

profile of v0, /device:TPU:1, one launch (start us, length us, event | category | flops | bytes accessed | tf_op | source)
XLA Modules:
  0.0 250.5 jit_solution(5828033538453089363)
XLA Ops:
  0.0 1.4 copy.68
  2.0 2.2 reduce.18
  5.0 8.5 %all-to-all-start.1 = ((bf16[16,2,4096]{2,1,0:T(2,128)(2,1)}), bf16[16,2,4096]{2,1,0:T(2,128)(2,1)}, u32[]{:S(2)}, u32[]{:S(2)}) async-start(bf16[16,2,4096]{2,1,0:T(2,128)(2,1)} %reshape.330), calls=%async_computation.1 | async-start | bytes 524288 | tf_op jit(solution)/shard_map/all_to_all | solution.py:82
  16.1 2.0 pad_maximum_fusion
  18.1 2.9 %all-to-all-done.1 = bf16[16,2,4096]{2,1,0:T(2,128)(2,1)} async-done(((bf16[16,2,4096]{2,1,0:T(2,128)(2,1)}), bf16[16,2,4096]{2,1,0:T(2,128)(2,1)}, u32[]{:S(2)}, u32[]{:S(2)}) %all-to-all-start.1) | async-done | bytes 262176 | tf_op jit(solution)/shard_map/all_to_all | solution.py:82
  21.1 4.0 %all-to-all-start = ((bf16[2,128,1024]{1,0,2:T(2,128)(2,1)}), bf16[2,128,1024]{1,0,2:T(2,128)(2,1)S(1)}, u32[]{:S(2)}, u32[]{:S(2)}) async-start(bf16[2,128,1024]{1,0,2:T(2,128)(2,1)} %pad_maximum_fusion), calls=%async_computation | async-start | bytes 1048576 | tf_op jit(solution)/shard_map/all_to_all | solution.py:12
  26.0 2.2 reshape.331
  28.4 6.5 %all-to-all-done = bf16[2,128,1024]{1,0,2:T(2,128)(2,1)S(1)} async-done(((bf16[2,128,1024]{1,0,2:T(2,128)(2,1)}), bf16[2,128,1024]{1,0,2:T(2,128)(2,1)S(1)}, u32[]{:S(2)}, u32[]{:S(2)}) %all-to-all-start) | async-done | bytes 524320 | tf_op jit(solution)/shard_map/all_to_all | solution.py:12
  37.6 0.9 fusion.86
  40.6 1.1 fusion.85
  42.3 0.8 fusion.32
  44.0 12.9 %reduce.19 = bf16[2048,64]{1,0:T(8,128)(2,1)} reduce(bf16[2048,1,64]{2,1,0:T(2,128)(2,1)S(1)} %bitcast.230, bf16[]{:T(256)} %broadcast.177), dimensions={1}, to_apply=%bitcast.196.reduce_sub_computation | reduce | bytes 524290
  56.9 2.1 reshape.332
  59.0 3.7 %all-to-all-start.2 = ((bf16[16,2,4096]{2,1,0:T(2,128)(2,1)}), bf16[16,2,4096]{2,1,0:T(2,128)(2,1)S(1)}, u32[]{:S(2)}, u32[]{:S(2)}) async-start(bf16[16,2,4096]{2,1,0:T(2,128)(2,1)} %reshape.332), calls=%async_computation.2 | async-start | bytes 524288 | tf_op jit(solution)/shard_map/all_to_all | solution.py:84
  62.7 1.2 fusion.47
  64.1 6.2 %all-to-all-done.2 = bf16[16,2,4096]{2,1,0:T(2,128)(2,1)S(1)} async-done(((bf16[16,2,4096]{2,1,0:T(2,128)(2,1)}), bf16[16,2,4096]{2,1,0:T(2,128)(2,1)S(1)}, u32[]{:S(2)}, u32[]{:S(2)}) %all-to-all-start.2) | async-done | bytes 262176 | tf_op jit(solution)/shard_map/all_to_all | solution.py:84
  71.7 3.1 %multiply_reduce_fusion.2 = (f32[128]{0:T(128)S(1)}, f32[128,2048]{1,0:T(8,128)S(1)}) fusion(bf16[128,1024]{0,1:T(8,128)(2,1)S(1)} %bitcast.235, bf16[1024,2048]{1,0:T(8,128)(2,1)} %param.21), kind=kOutput, calls=%fused_computation.58 | convolution fusion | flops 537395072 | bytes 5505536 | tf_op jit(solution)/shard_map/dot_general | solution.py:85
  75.6 0.8 copy-done.1
  76.4 2.4 broadcast_in_dim.29
  78.8 4.0 %reshape.323 = bf16[512,2048]{1,0:T(8,128)(2,1)} reshape(bf16[128,4,2048]{2,1,0:T(4,128)(2,1)} %broadcast_in_dim.29) | data formatting | bytes 4194304 | tf_op jit(solution)/shard_map/reshape | solution.py:110
  82.8 7.2 %scatter_custom_fusion = bf16[1024,2048]{1,0:T(8,128)(2,1)} fusion(s32[512]{0:T(512)S(1)} %bitcast.257, bf16[512,2048]{1,0:T(8,128)(2,1)} %reshape.323, bf16[]{:T(256)} %constant.10.clone.1), kind=kCustom, calls=%fused_computation.31 | custom fusion | bytes 4194816 | tf_op jit(solution)/shard_map/scatter | solution.py:112
  90.0 62.3 %all_to_all.55 = bf16[128,8,2048]{2,1,0:T(8,128)(2,1)S(1)} all-to-all(bf16[128,8,2048]{2,1,0:T(8,128)(2,1)} %bitcast.224), channel_id=1, replica_groups=mesh['sp'=16,'dp'=8] {'sp','dp'}, dimensions={0} | all-to-all | bytes 8388608 | tf_op jit(solution)/shard_map/all_to_all | solution.py:114
  152.3 2.0 copy-done.3
  154.2 3.7 %fusion.2 = f32[1024,512]{1,0:T(8,128)} fusion(bf16[128,8,2048]{2,1,0:T(8,128)(2,1)S(1)} %all_to_all.55, bf16[1,2048,512]{2,1,0:T(8,128)(2,1)S(1)} %copy-done.13), kind=kOutput, calls=%fused_computation.4 | convolution fusion | flops 2147483648 | bytes 8388608 | tf_op jit(solution)/shard_map/dot_general | solution.py:58
  158.0 10.0 %convert_bitcast_fusion = bf16[128,8,2048]{2,1,0:T(8,128)(2,1)} fusion(bf16[1,512,2048]{2,1,0:T(8,128)(2,1)S(1)} %copy-done, f32[1024,512]{1,0:T(8,128)} %fusion.2, bf16[1,2048,512]{2,1,0:T(8,128)(2,1)} %param.27, bf16[128,8,2048]{2,1,0:T(8,128)(2,1)} %copy-done.3), kind=kOutput, calls=%fused_computation.8 | convolution fusion | flops 4300210176 | bytes 14680064 | tf_op jit(solution)/shard_map/dot_general | solution.py:123
  167.9 6.0 %all-to-all-start.4 = ((bf16[128,8,2048]{2,1,0:T(8,128)(2,1)}), bf16[128,8,2048]{2,1,0:T(8,128)(2,1)}, u32[]{:S(2)}, u32[]{:S(2)}) async-start(bf16[128,8,2048]{2,1,0:T(8,128)(2,1)} %convert_bitcast_fusion), calls=%async_computation.4 | async-start | bytes 8388608 | tf_op jit(solution)/shard_map/all_to_all | solution.py:126
  174.1 2.2 fusion.89
  176.3 50.3 %all-to-all-done.4 = bf16[128,8,2048]{2,1,0:T(8,128)(2,1)} async-done(((bf16[128,8,2048]{2,1,0:T(8,128)(2,1)}), bf16[128,8,2048]{2,1,0:T(8,128)(2,1)}, u32[]{:S(2)}, u32[]{:S(2)}) %all-to-all-start.4) | async-done | bytes 4194336 | tf_op jit(solution)/shard_map/all_to_all | solution.py:126
  226.7 8.0 %gather_fusion = bf16[512,2048]{1,0:T(8,128)(2,1)} fusion(bf16[1024,2048]{1,0:T(8,128)(2,1)} %bitcast.42, s32[1024]{0:T(1024)S(1)} %pad_clamp_fusion), kind=kCustom, calls=%fused_computation | custom fusion | bytes 4196352 | tf_op jit(solution)/shard_map/gather | solution.py:129
  234.6 4.8 %reshape.310 = f32[128,4,2048]{2,1,0:T(4,128)} reshape(bf16[512,2048]{1,0:T(8,128)(2,1)} %gather_fusion) | data formatting | bytes 6291456 | tf_op jit(solution)/shard_map/convert_element_type | solution.py:130
  239.4 6.3 %multiply_reduce_fusion = f32[128,2048]{1,0:T(8,128)} fusion(f32[128,4,2048]{2,1,0:T(4,128)} %reshape.310, f32[128,4]{1,0:T(8,128)S(1)} %copy.87), kind=kLoop, calls=%fused_computation.7 | loop fusion | flops 1835008 | bytes 5244928 | tf_op jit(solution)/shard_map/reduce_sum | solution.py:131
  245.7 4.5 %fusion.12 = bf16[1,128,2048]{2,1,0:T(8,128)(2,1)} fusion(f32[128,2048]{1,0:T(8,128)} %multiply_reduce_fusion, bf16[512,2048]{1,0:T(8,128)(2,1)} %param.31, bf16[128,2048]{1,0:T(8,128)(2,1)} %copy-done.1, bf16[2048,512]{1,0:T(8,128)(2,1)} %param.30, f32[128,512]{1,0:T(8,128)S(1)} %fusion.89, f32[128]{0:T(128)S(1)} %add_rsqrt_fusion.1, ...), kind=kOutput, calls=%fused_computation.25 | convolution fusion | flops 539099136 | bytes 8135168 | tf_op jit(solution)/shard_map/dot_general | solution.py:96
  (91 shorter events, 13.6 us)
Async XLA Ops:
  0.0 158.0 %copy-start = (bf16[1,512,2048]{2,1,0:T(8,128)(2,1)S(1)}, bf16[1,512,2048]{2,1,0:T(8,128)(2,1)}, u32[]{:S(2)}) copy-start(bf16[1,512,2048]{2,1,0:T(8,128)(2,1)} %param.28) | copy-start | bytes 6291460
  0.0 14.1 %copy-start.9 = (s32[1,128,4]{1,2,0:T(4,128)S(1)}, s32[1,128,4]{1,2,0:T(4,128)}, u32[]{:S(2)}) copy-start(s32[1,128,4]{1,2,0:T(4,128)} %param.24) | copy-start | bytes 6148
  0.0 14.8 %copy-start.4 = (bf16[1,128,1024]{2,1,0:T(8,128)(2,1)S(1)}, bf16[1,128,1024]{2,1,0:T(8,128)(2,1)}, u32[]{:S(2)}) copy-start(bf16[1,128,1024]{2,1,0:T(8,128)(2,1)} %param.18) | copy-start | bytes 786436
  0.0 15.2 %copy-start.5 = (bf16[1,128,1024]{2,1,0:T(8,128)(2,1)S(1)}, bf16[1,128,1024]{2,1,0:T(8,128)(2,1)}, u32[]{:S(2)}) copy-start(bf16[1,128,1024]{2,1,0:T(8,128)(2,1)} %param.19) | copy-start | bytes 786436
  0.0 15.6 %copy-start.7 = (f32[1,1,2048]{2,1,0:T(1,128)S(1)}, f32[1,1,2048]{2,1,0:T(1,128)}, u32[]{:S(2)}) copy-start(f32[1,1,2048]{2,1,0:T(1,128)} %param.20) | copy-start | bytes 24580
  5.0 16.1 %all-to-all-start.1 = ((bf16[16,2,4096]{2,1,0:T(2,128)(2,1)}), bf16[16,2,4096]{2,1,0:T(2,128)(2,1)}, u32[]{:S(2)}, u32[]{:S(2)}) async-start(bf16[16,2,4096]{2,1,0:T(2,128)(2,1)} %reshape.330), calls=%async_computation.1 | async-start | bytes 524288 | tf_op jit(solution)/shard_map/all_to_all | solution.py:82
  21.1 13.8 %all-to-all-start = ((bf16[2,128,1024]{1,0,2:T(2,128)(2,1)}), bf16[2,128,1024]{1,0,2:T(2,128)(2,1)S(1)}, u32[]{:S(2)}, u32[]{:S(2)}) async-start(bf16[2,128,1024]{1,0,2:T(2,128)(2,1)} %pad_maximum_fusion), calls=%async_computation | async-start | bytes 1048576 | tf_op jit(solution)/shard_map/all_to_all | solution.py:12
  35.0 1.0 copy-start.12
  43.2 20.7 %copy-start.10 = (s32[1,128,4]{1,2,0:T(4,128)S(1)}, s32[1,128,4]{1,2,0:T(4,128)}, u32[]{:S(2)}) copy-start(s32[1,128,4]{1,2,0:T(4,128)} %broadcast_multiply_fusion) | copy-start | bytes 6148
  59.0 11.3 %all-to-all-start.2 = ((bf16[16,2,4096]{2,1,0:T(2,128)(2,1)}), bf16[16,2,4096]{2,1,0:T(2,128)(2,1)S(1)}, u32[]{:S(2)}, u32[]{:S(2)}) async-start(bf16[16,2,4096]{2,1,0:T(2,128)(2,1)} %reshape.332), calls=%async_computation.2 | async-start | bytes 524288 | tf_op jit(solution)/shard_map/all_to_all | solution.py:84
  71.7 3.1 %copy-start.2 = (bf16[1,128,2048]{2,1,0:T(8,128)(2,1)S(1)}, bf16[1,128,2048]{2,1,0:T(8,128)(2,1)}, u32[]{:S(2)}) copy-start(bf16[1,128,2048]{2,1,0:T(8,128)(2,1)} %param.16) | copy-start | bytes 1572868
  71.7 3.1 %copy-start.6 = (f32[2048]{0:T(1024)S(1)}, f32[2048]{0:T(1024)}, u32[]{:S(2)}) copy-start(f32[2048]{0:T(1024)} %param.22) | copy-start | bytes 24580
  71.7 3.5 %copy-start.8 = (f32[2048]{0:T(1024)S(1)}, f32[2048]{0:T(1024)}, u32[]{:S(2)}) copy-start(f32[2048]{0:T(1024)} %param.23) | copy-start | bytes 24580
  75.6 0.8 copy-start.1
  90.0 64.2 %copy-start.13 = (bf16[1,2048,512]{2,1,0:T(8,128)(2,1)S(1)}, bf16[1,2048,512]{2,1,0:T(8,128)(2,1)}, u32[]{:S(2)}) copy-start(bf16[1,2048,512]{2,1,0:T(8,128)(2,1)} %param.26) | copy-start | bytes 6291460
  152.3 2.0 copy-start.3
  167.9 6.0 %copy-start.11 = (f32[1,128,4]{1,2,0:T(4,128)S(1)}, f32[1,128,4]{1,2,0:T(4,128)}, u32[]{:S(2)}) copy-start(f32[1,128,4]{1,2,0:T(4,128)} %param.25) | copy-start | bytes 6148
  167.9 58.7 %all-to-all-start.4 = ((bf16[128,8,2048]{2,1,0:T(8,128)(2,1)}), bf16[128,8,2048]{2,1,0:T(8,128)(2,1)}, u32[]{:S(2)}, u32[]{:S(2)}) async-start(bf16[128,8,2048]{2,1,0:T(8,128)(2,1)} %convert_bitcast_fusion), calls=%async_computation.4 | async-start | bytes 8388608 | tf_op jit(solution)/shard_map/all_to_all | solution.py:126
where the time goes:
time: 255 us; the launch traced here: 251 us
  waiting for transfers between devices  66 us (26%)
  blocking collectives  62.3 us (24%)
  local copies, waits for them, and re-layouts  41.9 us (16%)
  matrix products  28.8 us (11%)
  other arithmetic  28.6 us (11%)
  starting transfers between devices  22.2 us (9%)
    all_to_all x1, blocking collectives, shards(): lax.all_to_all(outgoing.reshape(expert_count, capacity, width), ('sp', 'd...  62.3 us
    all_to_all x1, waiting for transfers between devices, shards(): lax.all_to_all(finished.reshape(arrived.shape), ('sp', 'dp'), split_axis=...  50.3 us
    unnamed x2, other arithmetic  15.1 us
    unnamed x40, local copies, waits for them, and re-layouts  11.5 us
    dot_general x1, matrix products, shards(): jnp.dot(hidden, expert_down[0], preferred_element_type=jnp.float32)  9.96 us
    all_to_all x1, starting transfers between devices, shards(): lax.all_to_all(query_rows, 'sp', split_axis=2, concat_axis=1, tiled=True)  8.47 us
    gather x1, local copies, waits for them, and re-layouts, shards(): picked = received.reshape(expert_count * capacity, width)[slot_index]  7.96 us
    scatter x1, local copies, waits for them, and re-layouts, shards(): jnp.zeros((expert_count * capacity, width), jnp.bfloat16).at[slot_index]  7.21 us
  transfers between devices with their start and end apart: 4, of which 4 were waited for; matrix products, arithmetic and copies ran while one was open for 5% of the time, Pallas kernels for 0%

commit v1 on v0

v1 whole, which is shorter than its diff:
```python
import functools

import jax
import jax.numpy as jnp
from jax import lax
from jax.experimental import pallas as pl
from jax.experimental.pallas import tpu as pltpu
from jax.sharding import PartitionSpec as P

HEAD_DIM = 64
MESH = pl.DeviceIdType.MESH
PEERS = 128
SLOTS = 8
GROUPS = 4
PER = PEERS // GROUPS
F32 = jnp.float32
BF16 = jnp.bfloat16


def sent_together(arrays, axis, split_dim, concat_dim, along):
    both = jnp.concatenate(arrays, axis=along)
    out, at, gathered = (
        lax.all_to_all(both, axis, split_axis=split_dim, concat_axis=concat_dim, tiled=True),
        0,
        [],
    )
    for a in arrays:
        gathered.append(lax.slice_in_dim(out, at, at + a.shape[along], axis=along))
        at += a.shape[along]
    return tuple(gathered)


def attend(query_all, key_all, value_all, gate_sums):
    length = query_all.shape[1]
    head_count = gate_sums.shape[1]
    score_scale = HEAD_DIM ** (-0.5)
    query_heads = query_all[0].reshape(length, head_count, HEAD_DIM)
    key_heads = key_all[0].reshape(length, head_count, HEAD_DIM)
    value_heads = value_all[0].reshape(length, head_count, HEAD_DIM)
    sums_local = gate_sums[0]
    block_rows = min(512, length)
    pieces = []
    for block_index in range(length // block_rows):
        start = block_index * block_rows
        block_end = start + block_rows
        scores = (
            jnp.einsum(
                "qhd,khd->hqk",
                query_heads[start:block_end],
                key_heads[:block_end],
                preferred_element_type=jnp.float32,
            )
            * score_scale
        )
        scores = scores + sums_local[:, start:block_end, None] - sums_local[:, None, :block_end]
        causal_mask = jnp.arange(block_end)[None, :] <= jnp.arange(start, block_end)[:, None]
        scores = jnp.where(causal_mask[None], scores, -jnp.inf)
        peak = jnp.max(scores, axis=2, keepdims=True)
        weights = jnp.exp(scores - peak)
        weights = (weights / jnp.sum(weights, axis=2, keepdims=True)).astype(jnp.bfloat16)
        mixed_heads = jnp.einsum(
            "hqk,khd->qhd", weights, value_heads[:block_end], preferred_element_type=jnp.float32
        ).astype(jnp.bfloat16)
        pieces.append(mixed_heads.reshape(block_rows, head_count * HEAD_DIM))
    return jnp.concatenate(pieces, axis=0)[None]


def shift_of(k):
    group, core, dz, dx = k // 32, (k // 16) % 2, (k // 4) % 4, k % 4
    return dz, dx, (group + dz + dx) % 4, core


def moved(shift, sign):
    dz, dx, dy, dc = shift
    sp, dp = lax.axis_index("sp"), lax.axis_index("dp")
    z = (sp // 4 + sign * dz + 4) % 4
    x = (sp % 4 + sign * dx + 4) % 4
    y = (dp // 2 + sign * dy + 4) % 4
    c = (dp % 2 + dc) % 2
    return z * 4 + x, y * 2 + c


def dot(a, b):
    return jnp.dot(a, b, preferred_element_type=F32)


def moe_kernel(
    h_ref, res_ref, place_ref, mixw_ref, mixg_ref, ffng_ref,
    wo_any, sg_any, su_any, sd_any, eg_any, eu_any, ed_any,
    o_ref,
    wo, sg, su, sd, eg, eu, ed, outgoing, arrived, result, received, acc, normed,
    wsem, ready, out_s, out_r, ret_s, ret_r,
):
    loads = [
        pltpu.make_async_copy(src, dst, wsem.at[i])
        for i, (src, dst) in enumerate(
            [(wo_any, wo), (sg_any, sg), (su_any, su), (sd_any, sd), (eg_any, eg), (eu_any, eu), (ed_any, ed)]
        )
    ]
    for c in loads:
        c.start()
    barrier = pltpu.get_barrier_semaphore()

    def hello_sp(k, _):
        pl.semaphore_signal(barrier, inc=1, device_id=moved((k // 4, k % 4, 0, 0), 1), device_id_type=MESH)
        return 0

    def hello_dp(k, _):
        pl.semaphore_signal(barrier, inc=1, device_id=moved((0, 0, k // 2, k % 2), 1), device_id_type=MESH)
        return 0

    def row_ready(k, _):
        pl.semaphore_signal(ready, inc=1, device_id=moved((0, 0, k // 2, k % 2), 1), device_id_type=MESH)
        return 0

    lax.fori_loop(1, 16, hello_sp, 0)
    lax.fori_loop(1, 8, hello_dp, 0)

    loads[0].wait()
    projected = dot(h_ref[...], wo[...])
    pl.semaphore_wait(barrier, 22)
    lax.fori_loop(1, 8, row_ready, 0)
    mixed = res_ref[...].astype(F32) + mixg_ref[...] * projected * lax.rsqrt(
        jnp.mean(projected * projected, axis=1, keepdims=True) + 1e-06
    )
    acc[...] = mixed
    normed[...] = (
        ffng_ref[...] * mixed * lax.rsqrt(jnp.mean(mixed * mixed, axis=1, keepdims=True) + 1e-06)
    ).astype(BF16)
    pl.semaphore_wait(ready, 7)

    def out_copy(k, c):
        return pltpu.make_async_remote_copy(
            src_ref=outgoing.at[k], dst_ref=arrived.at[k], send_sem=out_s.at[c], recv_sem=out_r.at[c],
            device_id=moved(shift_of(k), 1), device_id_type=MESH,
        )

    def ret_copy(k, c):
        return pltpu.make_async_remote_copy(
            src_ref=result.at[k], dst_ref=received.at[k], send_sem=ret_s.at[c], recv_sem=ret_r.at[c],
            device_id=moved(shift_of(k), -1), device_id_type=MESH,
        )

    def send_group(copy, c):
        def one(k, _):
            copy(k, c).start()
            return 0

        lax.fori_loop(jnp.where(c == 0, 1, c * PER), (c + 1) * PER, one, 0)

    def wait_group(ref, sem, c):
        @pl.when(c == 0)
        def _():
            part = ref.at[pl.ds(1, PER - 1)]
            pltpu.make_async_copy(part, part, sem.at[0]).wait()

        @pl.when(c > 0)
        def _():
            part = ref.at[pl.ds(c * PER, PER)]
            pltpu.make_async_copy(part, part, sem.at[c]).wait()

    def pack(c, _):
        rows = dot(place_ref[pl.ds(pl.multiple_of(c * PER * SLOTS, PER * SLOTS), PER * SLOTS), :], normed[...])
        outgoing[pl.ds(c * PER, PER)] = rows.reshape(PER, SLOTS, rows.shape[1]).astype(BF16)

        @pl.when(c == 0)
        def _():
            arrived[0] = outgoing[0]

        send_group(out_copy, c)
        return 0

    lax.fori_loop(0, GROUPS, pack, 0)

    for c in loads[1:4]:
        c.wait()
    gate = dot(normed[...], sg[...])
    up = dot(normed[...], su[...])
    hidden = (gate / (1.0 + jnp.exp(-gate)) * up).astype(BF16)
    acc[...] += dot(hidden, sd[...])
    for c in loads[4:]:
        c.wait()

    def expert(c, _):
        wait_group(arrived, out_r, c)
        rows = arrived[pl.ds(c * PER, PER)].astype(F32).reshape(PER * SLOTS, arrived.shape[2]).astype(BF16)
        g = dot(rows, eg[...])
        u = dot(rows, eu[...])
        hid = (g / (1.0 + jnp.exp(-g)) * u).astype(BF16)
        y = dot(hid, ed[...])
        result[pl.ds(c * PER, PER)] = y.reshape(PER, SLOTS, y.shape[1]).astype(BF16)

        @pl.when(c == 0)
        def _():
            received[0] = result[0]

        send_group(ret_copy, c)
        return 0

    lax.fori_loop(0, GROUPS, expert, 0)

    def combine(c, _):
        wait_group(received, ret_r, c)
        rows = received[pl.ds(c * PER, PER)].astype(F32).reshape(PER * SLOTS, received.shape[2]).astype(BF16)
        w = mixw_ref[pl.ds(pl.multiple_of(c * PER * SLOTS, PER * SLOTS), PER * SLOTS), :]
        hi = w.astype(BF16)
        lo = (w - hi.astype(F32)).astype(BF16)
        dims = (((0,), (0,)), ((), ()))
        acc[...] += lax.dot_general(hi, rows, dims, preferred_element_type=F32) + lax.dot_general(
            lo, rows, dims, preferred_element_type=F32
        )
        return 0

    lax.fori_loop(0, GROUPS, combine, 0)
    o_ref[...] = acc[...].astype(BF16)

    def drain(c, _):
        wait_group(outgoing, out_s, c)
        wait_group(result, ret_s, c)
        return 0

    lax.fori_loop(0, GROUPS, drain, 0)


def moe_layer(heads, residual, place, mixw, mix_gain, ffn_gain, wo, sg, su, sd, eg, eu, ed):
    tok, width = residual.shape
    vm, hbm = pl.BlockSpec(memory_space=pltpu.VMEM), pl.BlockSpec(memory_space=pl.ANY)
    weights = (wo, sg, su, sd, eg, eu, ed)
    boxes = pltpu.VMEM((PEERS, SLOTS, width), BF16)
    return pl.pallas_call(
        moe_kernel,
        out_shape=jax.ShapeDtypeStruct((tok, width), BF16),
        in_specs=[vm] * 6 + [hbm] * 7,
        out_specs=vm,
        scratch_shapes=[pltpu.VMEM(w.shape, w.dtype) for w in weights]
        + [boxes] * 4
        + [pltpu.VMEM((tok, width), F32), pltpu.VMEM((tok, width), BF16)]
        + [pltpu.SemaphoreType.DMA((7,)), pltpu.SemaphoreType.REGULAR]
        + [pltpu.SemaphoreType.DMA((GROUPS,))] * 4,
        compiler_params=pltpu.CompilerParams(
            collective_id=1, has_side_effects=True, vmem_limit_bytes=60 * 2**20
        ),
        name="moe_layer",
    )(heads, residual, place, mixw, mix_gain[None], ffn_gain[None], *weights)


def routing(expert_ids, route_weights):
    tok, top = expert_ids.shape
    sp, dp = moved(shift_of(jnp.arange(PEERS, dtype=jnp.int32)), 1)
    peer = sp * 8 + dp
    hit = expert_ids.T[:, None, :] == peer[None, :, None]
    named = jnp.any(hit, axis=0)
    weight = jnp.sum(jnp.where(hit, route_weights.T[:, None, :], 0.0), axis=0)
    earlier = jnp.arange(tok)[:, None] < jnp.arange(tok)[None, :]
    rank = jnp.dot(named.astype(BF16), earlier.astype(BF16), preferred_element_type=F32).astype(jnp.int32)
    at = named[:, None, :] & (rank[:, None, :] == jnp.arange(SLOTS, dtype=jnp.int32)[None, :, None])
    place = at.astype(BF16).reshape(PEERS * SLOTS, tok)
    mixw = jnp.where(at, weight[:, None, :], 0.0).reshape(PEERS * SLOTS, tok)
    return place, mixw


def shards(
    residual_in,
    query_rows,
    key_rows,
    value_rows,
    gate_sums,
    out_weight,
    mix_gain,
    ffn_gain,
    expert_ids,
    route_weights,
    expert_gate,
    expert_up,
    expert_down,
    shared_gate,
    shared_up,
    shared_down,
):
    place, mixw = routing(expert_ids[0], route_weights[0])
    key_all, value_all = sent_together((key_rows, value_rows), "sp", 2, 1, 0)
    query_all = lax.all_to_all(query_rows, "sp", split_axis=2, concat_axis=1, tiled=True)
    attended = attend(query_all, key_all, value_all, gate_sums)
    returned = lax.all_to_all(attended, "sp", split_axis=1, concat_axis=2, tiled=True)
    return moe_layer(
        returned[0], residual_in[0], place, mixw, mix_gain, ffn_gain, out_weight,
        shared_gate, shared_up, shared_down, expert_gate[0], expert_up[0], expert_down[0],
    )[None]


def solution(mesh):
    return jax.shard_map(
        shards,
        mesh=mesh,
        in_specs=(
            P("dp", "sp", None),
            P("dp", "sp", None),
            P("dp", "sp", None),
            P("dp", "sp", None),
            P("dp", "sp", None),
            P(),
            P(),
            P(),
            P("dp", "sp", None),
            P("dp", "sp", None),
            P(("sp", "dp"), None, None),
            P(("sp", "dp"), None, None),
            P(("sp", "dp"), None, None),
            P(),
            P(),
            P(),
        ),
        out_specs=P("dp", "sp", None),
        check_vma=False,
    )
```

time: 255 us -> 189 us (0.74)
  the two profiles are of different devices: /device:TPU:1 before, /device:TPU:2 now
where the time goes in v1:
time: 189 us
  Pallas kernels  115 us (61%)
  other arithmetic  19.7 us (10%)
  starting transfers between devices  18.5 us (10%)
  waiting for transfers between devices  16.1 us (9%)
  local copies, waits for them, and re-layouts  13.4 us (7%)
  matrix products  5.46 us (3%)
    pallas_call x1, Pallas kernels, moe_layer(): pl.pallas_call(moe_kernel, out_shape=jax.ShapeDtypeStruct((tok, width), B...  115 us
    unnamed x2, other arithmetic  13.9 us
    all_to_all x1, starting transfers between devices, shards(): lax.all_to_all(query_rows, 'sp', split_axis=2, concat_axis=1, tiled=True)  8.32 us
    unnamed x19, local copies, waits for them, and re-layouts  8.25 us
    all_to_all x1, waiting for transfers between devices, sent_together(): lax.all_to_all(both, axis, split_axis=split_dim, concat_axis=concat_dim,...  7.98 us
    all_to_all x1, waiting for transfers between devices, shards(): lax.all_to_all(attended, 'sp', split_axis=1, concat_axis=2, tiled=True)  6.32 us
    all_to_all x1, starting transfers between devices, sent_together(): lax.all_to_all(both, axis, split_axis=split_dim, concat_axis=concat_dim,...  5.4 us
    all_to_all x1, starting transfers between devices, shards(): lax.all_to_all(attended, 'sp', split_axis=1, concat_axis=2, tiled=True)  4.77 us
  transfers between devices with their start and end apart: 3, of which 3 were waited for; matrix products, arithmetic and copies ran while one was open for 4% of the time, Pallas kernels for 0%

profile of v1, /device:TPU:2, one launch (start us, length us, event | category | flops | bytes accessed | tf_op | source)
XLA Modules:
  0.0 188.6 jit_solution(14131608489020900703)
XLA Ops:
  0.0 1.3 copy.78
  1.3 0.6 broadcast.393
  1.9 2.2 %reduce.18 = bf16[1024,128]{1,0:T(8,128)(2,1)S(1)} reduce(bf16[1024,1,128]{2,1,0:T(2,128)(2,1)S(1)} %bitcast.202, bf16[]{:T(256)} %broadcast.393), dimensions={1}, to_apply=%bitcast.173.reduce_sub_computation | reduce | bytes 524290
  4.1 0.8 reshape.362
  4.8 8.3 %all-to-all-start.1 = ((bf16[16,2,4096]{2,1,0:T(2,128)(2,1)}), bf16[16,2,4096]{2,1,0:T(2,128)(2,1)S(1)}, u32[]{:S(2)}, u32[]{:S(2)}) async-start(bf16[16,2,4096]{2,1,0:T(2,128)(2,1)} %reshape.362), calls=%async_computation.1 | async-start | bytes 524288 | tf_op jit(solution)/shard_map/all_to_all | solution.py:282
  13.2 0.7 fusion.70
  13.9 0.7 slice_reduce_fusion
  14.7 1.3 copy.73
  16.4 2.0 %pad_maximum_fusion = bf16[2,128,1024]{1,0,2:T(2,128)(2,1)} fusion(bf16[1,128,1024]{1,0,2:T(2,128)(2,1)S(1)} %copy.74, bf16[1,128,1024]{1,0,2:T(2,128)(2,1)S(1)} %copy.73), kind=kLoop, calls=%fused_computation.39 | loop fusion | flops 1048576 | bytes 1048576 | tf_op jit(solution)/shard_map/concatenate | solution.py:21
  18.7 1.8 all-to-all-done.1
  20.5 5.4 %all-to-all-start = ((bf16[2,128,1024]{1,0,2:T(2,128)(2,1)}), bf16[2,128,1024]{1,0,2:T(2,128)(2,1)S(1)}, u32[]{:S(2)}, u32[]{:S(2)}) async-start(bf16[2,128,1024]{1,0,2:T(2,128)(2,1)} %pad_maximum_fusion), calls=%async_computation | async-start | bytes 1048576 | tf_op jit(solution)/shard_map/all_to_all | solution.py:23
  26.0 0.9 fusion.21.place_ref
  27.5 8.0 %all-to-all-done = bf16[2,128,1024]{1,0,2:T(2,128)(2,1)S(1)} async-done(((bf16[2,128,1024]{1,0,2:T(2,128)(2,1)}), bf16[2,128,1024]{1,0,2:T(2,128)(2,1)S(1)}, u32[]{:S(2)}, u32[]{:S(2)}) %all-to-all-start) | async-done | bytes 524320 | tf_op jit(solution)/shard_map/all_to_all | solution.py:23
  36.7 0.7 fusion.73
  37.7 0.5 fusion.17
  38.2 0.9 fusion.72
  39.1 0.5 fusion.5
  39.6 0.7 fusion.16
  41.2 1.1 fusion.71
  42.3 0.6 fusion
  42.9 0.8 fusion.15
  43.8 0.7 copy.89
  44.5 11.7 %reduce.19 = bf16[2048,64]{1,0:T(8,128)(2,1)S(1)} reduce(bf16[2048,1,64]{2,1,0:T(2,128)(2,1)S(1)} %bitcast.199, bf16[]{:T(256)} %broadcast.393), dimensions={1}, to_apply=%bitcast.175.reduce_sub_computation | reduce | bytes 524290
  56.3 1.1 reshape.364
  57.4 4.8 %all-to-all-start.2 = ((bf16[16,2,4096]{2,1,0:T(2,128)(2,1)}), bf16[16,2,4096]{2,1,0:T(2,128)(2,1)S(1)}, u32[]{:S(2)}, u32[]{:S(2)}) async-start(bf16[16,2,4096]{2,1,0:T(2,128)(2,1)} %reshape.364), calls=%async_computation.2 | async-start | bytes 524288 | tf_op jit(solution)/shard_map/all_to_all | solution.py:284
  62.2 1.0 bitcast_select_fusion.2.mixw_ref
  63.2 6.3 %all-to-all-done.2 = bf16[16,2,4096]{2,1,0:T(2,128)(2,1)S(1)} async-done(((bf16[16,2,4096]{2,1,0:T(2,128)(2,1)}), bf16[16,2,4096]{2,1,0:T(2,128)(2,1)S(1)}, u32[]{:S(2)}, u32[]{:S(2)}) %all-to-all-start.2) | async-done | bytes 262176 | tf_op jit(solution)/shard_map/all_to_all | solution.py:284
  69.5 0.6 reshape.365
  70.2 0.6 copy.90
  70.9 0.9 copy.92.h_ref
  71.8 115.0 %moe_layer.1 = bf16[128,2048]{1,0:T(8,128)(2,1)} custom-call(bf16[128,1024]{1,0:T(8,128)(2,1)} %copy.92.h_ref, bf16[128,2048]{1,0:T(8,128)(2,1)} %bitcast.210, bf16[1024,128]{1,0:T(8,128)(2,1)} %fusion.21.place_ref, f32[1024,128]{1,0:T(8,128)} %bitcast_select_fusion.2.mixw_ref, f32[1,2048]{1,0:T(1,128)} %bitcast.227, f32[1,2048]{1,0:T(1,128)} %bitcast.228, ...), custom_call_target="tpu_custom_call" | custom-call | tf_op jit(solution)/shard_map/moe_layer/pallas_call | solution.py:230
  186.7 1.9 copy.172
  (46 shorter events, 3.8 us)
Async XLA Ops:
  0.0 15.9 %copy-start = (bf16[1,128,1024]{2,1,0:T(8,128)(2,1)S(1)}, bf16[1,128,1024]{2,1,0:T(8,128)(2,1)}, u32[]{:S(2)}) copy-start(bf16[1,128,1024]{2,1,0:T(8,128)(2,1)} %param.19) | copy-start | bytes 786436
  0.0 18.4 %copy-start.2 = (s32[1,128,4]{1,2,0:T(4,128)S(1)}, s32[1,128,4]{1,2,0:T(4,128)}, u32[]{:S(2)}) copy-start(s32[1,128,4]{1,2,0:T(4,128)} %param.24) | copy-start | bytes 6148
  1.3 24.6 %copy-start.1 = (f32[1,1,2048]{2,1,0:T(1,128)S(1)}, f32[1,1,2048]{2,1,0:T(1,128)}, u32[]{:S(2)}) copy-start(f32[1,1,2048]{2,1,0:T(1,128)} %param.20) | copy-start | bytes 24580
  4.8 15.7 %all-to-all-start.1 = ((bf16[16,2,4096]{2,1,0:T(2,128)(2,1)}), bf16[16,2,4096]{2,1,0:T(2,128)(2,1)S(1)}, u32[]{:S(2)}, u32[]{:S(2)}) async-start(bf16[16,2,4096]{2,1,0:T(2,128)(2,1)} %reshape.362), calls=%async_computation.1 | async-start | bytes 524288 | tf_op jit(solution)/shard_map/all_to_all | solution.py:282
  20.5 15.0 %all-to-all-start = ((bf16[2,128,1024]{1,0,2:T(2,128)(2,1)}), bf16[2,128,1024]{1,0,2:T(2,128)(2,1)S(1)}, u32[]{:S(2)}, u32[]{:S(2)}) async-start(bf16[2,128,1024]{1,0,2:T(2,128)(2,1)} %pad_maximum_fusion), calls=%async_computation | async-start | bytes 1048576 | tf_op jit(solution)/shard_map/all_to_all | solution.py:23
  43.7 18.4 %copy-start.3 = (f32[1,128,4]{1,2,0:T(4,128)S(1)}, f32[1,128,4]{1,2,0:T(4,128)}, u32[]{:S(2)}) copy-start(f32[1,128,4]{1,2,0:T(4,128)} %param.25) | copy-start | bytes 6148
  57.4 12.2 %all-to-all-start.2 = ((bf16[16,2,4096]{2,1,0:T(2,128)(2,1)}), bf16[16,2,4096]{2,1,0:T(2,128)(2,1)S(1)}, u32[]{:S(2)}, u32[]{:S(2)}) async-start(bf16[16,2,4096]{2,1,0:T(2,128)(2,1)} %reshape.364), calls=%async_computation.2 | async-start | bytes 524288 | tf_op jit(solution)/shard_map/all_to_all | solution.py:284

commit v2 on v1

v2 whole, which is shorter than its diff:
```python
import jax
import jax.numpy as jnp
from jax import lax
from jax.experimental import pallas as pl
from jax.experimental.pallas import tpu as pltpu
from jax.sharding import PartitionSpec as P

HEAD_DIM = 64
MESH = pl.DeviceIdType.MESH
PEERS = 128
SLOTS = 8
GROUPS = 4
PER = PEERS // GROUPS
F32 = jnp.float32
BF16 = jnp.bfloat16


def shift_of(k):
    group, core, dz, dx = k // 32, (k // 16) % 2, (k // 4) % 4, k % 4
    return dz, dx, (group + dz + dx) % 4, core


def moved(shift, sign):
    dz, dx, dy, dc = shift
    sp, dp = lax.axis_index("sp"), lax.axis_index("dp")
    z = (sp // 4 + sign * dz + 4) % 4
    x = (sp % 4 + sign * dx + 4) % 4
    y = (dp // 2 + sign * dy + 4) % 4
    c = (dp % 2 + dc) % 2
    return z * 4 + x, y * 2 + c


def dot(a, b):
    return jnp.dot(a, b, preferred_element_type=F32)


def swap_matrix():
    r = lax.broadcasted_iota(jnp.int32, (256, 256), 0)
    c = lax.broadcasted_iota(jnp.int32, (256, 256), 1)
    from_row = jnp.where((c >= 64) & (c < 128), c + 64, jnp.where((c >= 128) & (c < 192), c - 64, c))
    return jnp.where(r == from_row, 1.0, 0.0).astype(BF16)


def lifted(pairs):
    r = lax.broadcasted_iota(jnp.int32, (128, 256), 0)
    c = lax.broadcasted_iota(jnp.int32, (128, 256), 1)
    out = jnp.zeros((128, 256), F32)
    for row, col, scale in pairs:
        out = jnp.where((c >= col) & (c < col + 64) & (r - row == c - col), scale, out)
    return out.astype(BF16)


def layer_kernel(
    q_ref, k_ref, v_ref, gate_ref, ids_ref, rw_ref, res_ref, mixg_ref, ffng_ref,
    wo_any, sg_any, su_any, sd_any, eg_any, eu_any, ed_any,
    o_ref,
    wo, sg, su, sd, eg, eu, ed, outgoing, arrived, result, received, acc, normed,
    qkv_out, qkv_in, q_all, k_all, v_all, scores, att_out, heads_in, heads, code, weight,
    wsem, ready, out_s, out_r, ret_s, ret_r, qkv_s, qkv_r, att_s, att_r,
):
    loads = [
        pltpu.make_async_copy(src, dst, wsem.at[i])
        for i, (src, dst) in enumerate(
            [(wo_any, wo), (sg_any, sg), (su_any, su), (sd_any, sd), (eg_any, eg), (eu_any, eu), (ed_any, ed)]
        )
    ]
    me = lax.axis_index("sp")
    barrier = pltpu.get_barrier_semaphore()

    def hello_sp(k, _):
        pl.semaphore_signal(barrier, inc=1, device_id=moved((k // 4, k % 4, 0, 0), 1), device_id_type=MESH)
        return 0

    def hello_dp(k, _):
        pl.semaphore_signal(barrier, inc=1, device_id=moved((0, 0, k // 2, k % 2), 1), device_id_type=MESH)
        return 0

    def row_ready(k, _):
        pl.semaphore_signal(ready, inc=1, device_id=moved((0, 0, k // 2, k % 2), 1), device_id_type=MESH)
        return 0

    lax.fori_loop(1, 16, hello_sp, 0)
    lax.fori_loop(1, 8, hello_dp, 0)
    for c in loads:
        c.start()

    swap = swap_matrix()
    for p in range(8):
        cols = slice(p * 128, (p + 1) * 128)
        qk = dot(jnp.concatenate([q_ref[:, cols], k_ref[:, cols]], axis=1), swap).astype(BF16)
        vv = dot(jnp.concatenate([v_ref[:64, cols], v_ref[64:, cols]], axis=1), swap).astype(BF16)
        for side in range(2):
            part = slice(side * 128, (side + 1) * 128)
            qkv_out[2 * p + side, :128, :] = qk[:, part]
            qkv_out[2 * p + side, 128:, :] = vv[:, part]
    qkv_in[me] = qkv_out[me]

    pl.semaphore_wait(barrier, 22)

    def send_qkv(k, _):
        to = moved((k // 4, k % 4, 0, 0), 1)
        pltpu.make_async_remote_copy(
            src_ref=qkv_out.at[to[0]], dst_ref=qkv_in.at[me], send_sem=qkv_s, recv_sem=qkv_r,
            device_id=to, device_id_type=MESH,
        ).start()
        return 0

    lax.fori_loop(1, 16, send_qkv, 0)

    kth = lax.broadcasted_iota(jnp.int32, (PEERS, 1), 0)
    dz, dx = (kth >> 2) & 3, kth & 3
    dy, dc = ((kth >> 5) + dz + dx) & 3, (kth >> 4) & 1
    dp = lax.axis_index("dp")
    peer = (
        (((me // 4 + dz) & 3) * 4 + ((me % 4 + dx) & 3)) * 8 + ((dp // 2 + dy) & 3) * 2 + ((dp % 2 + dc) & 1)
    )
    named = jnp.zeros((PEERS, PEERS), F32)
    share = jnp.zeros((PEERS, PEERS), F32)
    for j in range(ids_ref.shape[0]):
        hit = ids_ref[j : j + 1, :] == peer
        named = jnp.where(hit, 1.0, named)
        share = jnp.where(hit, rw_ref[j : j + 1, :], share)
    earlier = jnp.where(
        lax.broadcasted_iota(jnp.int32, (PEERS, PEERS), 0) < lax.broadcasted_iota(jnp.int32, (PEERS, PEERS), 1),
        1.0,
        0.0,
    ).astype(BF16)
    rank = dot(named.astype(BF16), earlier)
    code[...] = jnp.where(named > 0.5, rank, -1.0)
    weight[...] = share

    pltpu.make_async_copy(qkv_in.at[pl.ds(0, 15)], qkv_in.at[pl.ds(0, 15)], qkv_r).wait()

    split_qk = lifted([(0, 0, HEAD_DIM**-0.5), (64, 128, 1.0)])
    split_v = lifted([(0, 0, 1.0), (0, 64, 1.0), (64, 128, 1.0), (64, 192, 1.0)])
    for j in range(16):
        rows = slice(j * 128, (j + 1) * 128)
        qk = dot(qkv_in[j, :128, :], split_qk).astype(BF16)
        vv = dot(qkv_in[j, 128:, :], split_v).astype(BF16)
        q_all[rows, :] = qk[:, :128]
        k_all[rows, :] = qk[:, 128:]
        v_all[j * 128 : j * 128 + 64, :] = vv[:, :128]
        v_all[j * 128 + 64 : (j + 1) * 128, :] = vv[:, 128:]

    left = lax.broadcasted_iota(jnp.int32, (64, 128), 1) < 64
    ahead = lax.broadcasted_iota(jnp.int32, (256, 256), 1) - lax.broadcasted_iota(jnp.int32, (256, 256), 0)

    def att_copy(b):
        return pltpu.make_async_remote_copy(
            src_ref=att_out.at[b], dst_ref=heads_in.at[me], send_sem=att_s, recv_sem=att_r,
            device_id=(b, lax.axis_index("dp")), device_id_type=MESH,
        )

    def attend(step, _):
        turn = (me // 2 + step) % 8
        q = q_all[pl.ds(pl.multiple_of(turn * 256, 256), 256), :]
        for group in range(4):

            @pl.when(turn // 2 == group)
            def _():
                last = group * 512
                parts = [slice(c, c + 256) for c in range(0, last + 512, 256)]
                base = gate_ref[:, last : last + 1]
                top = None
                for part in parts:
                    s = lax.dot_general(
                        q, k_all[part, :], (((1,), (1,)), ((), ())), preferred_element_type=F32
                    ) + (base - gate_ref[:, part])
                    if part.start >= last:
                        s = jnp.where(ahead <= (turn % 2) * 256 - (part.start - last), s, -jnp.inf)
                    scores[:, part] = s
                    peak = jnp.maximum(s[:, :128], s[:, 128:])
                    top = peak if top is None else jnp.maximum(top, peak)
                top = jnp.max(top, axis=1, keepdims=True)
                total = None
                for part in parts:
                    e = jnp.exp(scores[:, part] - top)
                    scores[:, part] = e
                    both = e[:, :128] + e[:, 128:]
                    total = both if total is None else total + both
                inverse = 1.0 / jnp.sum(total, axis=1, keepdims=True)
                o = None
                for part in parts:
                    piece = dot((scores[:, part] * inverse).astype(BF16), v_all[part, :])
                    o = piece if o is None else o + piece
                o = o.astype(BF16)
                att_out[2 * turn] = jnp.where(left, o[:64], o[64:128])
                att_out[2 * turn + 1] = jnp.where(left, o[128:192], o[192:])

        for half in range(2):
            b = 2 * turn + half

            @pl.when(b != me)
            def _():
                att_copy(b).start()

            @pl.when(b == me)
            def _():
                heads_in[me] = att_out[me]

        return 0

    lax.fori_loop(0, 8, attend, 0)
    pltpu.make_async_copy(heads_in.at[pl.ds(0, 15)], heads_in.at[pl.ds(0, 15)], att_r).wait()
    lax.fori_loop(1, 8, row_ready, 0)
    for p in range(8):
        two = dot(jnp.concatenate([heads_in[2 * p], heads_in[2 * p + 1]], axis=1), swap).astype(BF16)
        heads[:64, p * 128 : (p + 1) * 128] = two[:, :128]
        heads[64:, p * 128 : (p + 1) * 128] = two[:, 128:]

    loads[0].wait()
    projected = dot(heads[...], wo[...])
    mixed = res_ref[...].astype(F32) + mixg_ref[...] * projected * lax.rsqrt(
        jnp.mean(projected * projected, axis=1, keepdims=True) + 1e-06
    )
    acc[...] = mixed
    normed[...] = (
        ffng_ref[...] * mixed * lax.rsqrt(jnp.mean(mixed * mixed, axis=1, keepdims=True) + 1e-06)
    ).astype(BF16)
    pl.semaphore_wait(ready, 7)

    def slots_of(values, c):
        part = pl.ds(pl.multiple_of(c * PER, PER), PER)
        r = lax.broadcasted_iota(jnp.int32, (PER, SLOTS, PEERS), 1).astype(F32)
        at = code[part, :][:, None, :] == r
        return jnp.where(at, values(part), 0.0).reshape(PER * SLOTS, PEERS)

    def out_copy(k, c):
        return pltpu.make_async_remote_copy(
            src_ref=outgoing.at[k], dst_ref=arrived.at[k], send_sem=out_s.at[c], recv_sem=out_r.at[c],
            device_id=moved(shift_of(k), 1), device_id_type=MESH,
        )

    def ret_copy(k, c):
        return pltpu.make_async_remote_copy(
            src_ref=result.at[k], dst_ref=received.at[k], send_sem=ret_s.at[c], recv_sem=ret_r.at[c],
            device_id=moved(shift_of(k), -1), device_id_type=MESH,
        )

    def send_group(copy, c):
        def one(k, _):
            copy(k, c).start()
            return 0

        lax.fori_loop(jnp.where(c == 0, 1, c * PER), (c + 1) * PER, one, 0)

    def wait_group(ref, sem, c):
        @pl.when(c == 0)
        def _():
            part = ref.at[pl.ds(1, PER - 1)]
            pltpu.make_async_copy(part, part, sem.at[0]).wait()

        @pl.when(c > 0)
        def _():
            part = ref.at[pl.ds(c * PER, PER)]
            pltpu.make_async_copy(part, part, sem.at[c]).wait()

    def pack(c, _):
        rows = dot(slots_of(lambda part: 1.0, c).astype(BF16), normed[...])
        outgoing[pl.ds(c * PER, PER)] = rows.reshape(PER, SLOTS, rows.shape[1]).astype(BF16)

        @pl.when(c == 0)
        def _():
            arrived[0] = outgoing[0]

        send_group(out_copy, c)
        return 0

    lax.fori_loop(0, GROUPS, pack, 0)

    for c in loads[1:4]:
        c.wait()
    gate = dot(normed[...], sg[...])
    up = dot(normed[...], su[...])
    hidden = (gate / (1.0 + jnp.exp(-gate)) * up).astype(BF16)
    acc[...] += dot(hidden, sd[...])
    for c in loads[4:]:
        c.wait()

    def expert(c, _):
        wait_group(arrived, out_r, c)
        rows = arrived[pl.ds(c * PER, PER)].astype(F32).reshape(PER * SLOTS, arrived.shape[2]).astype(BF16)
        g = dot(rows, eg[...])
        u = dot(rows, eu[...])
        hid = (g / (1.0 + jnp.exp(-g)) * u).astype(BF16)
        y = dot(hid, ed[...])
        result[pl.ds(c * PER, PER)] = y.reshape(PER, SLOTS, y.shape[1]).astype(BF16)

        @pl.when(c == 0)
        def _():
            received[0] = result[0]

        send_group(ret_copy, c)
        return 0

    lax.fori_loop(0, GROUPS, expert, 0)

    def combine(c, _):
        wait_group(received, ret_r, c)
        rows = received[pl.ds(c * PER, PER)].astype(F32).reshape(PER * SLOTS, received.shape[2]).astype(BF16)
        w = slots_of(lambda part: weight[part, :][:, None, :], c)
        hi = w.astype(BF16)
        lo = (w - hi.astype(F32)).astype(BF16)
        dims = (((0,), (0,)), ((), ()))
        acc[...] += lax.dot_general(hi, rows, dims, preferred_element_type=F32) + lax.dot_general(
            lo, rows, dims, preferred_element_type=F32
        )
        return 0

    lax.fori_loop(0, GROUPS, combine, 0)
    o_ref[...] = acc[...].astype(BF16)

    pltpu.make_async_copy(qkv_out.at[pl.ds(0, 15)], qkv_out.at[pl.ds(0, 15)], qkv_s).wait()
    pltpu.make_async_copy(att_out.at[pl.ds(0, 15)], att_out.at[pl.ds(0, 15)], att_s).wait()

    def drain(c, _):
        wait_group(outgoing, out_s, c)
        wait_group(result, ret_s, c)
        return 0

    lax.fori_loop(0, GROUPS, drain, 0)


def layer(q, k, v, gates, ids, rw, residual, mix_gain, ffn_gain, *weights):
    tok, width = residual.shape
    length = gates.shape[1]
    vm, hbm = pl.BlockSpec(memory_space=pltpu.VMEM), pl.BlockSpec(memory_space=pl.ANY)
    boxes = pltpu.VMEM((PEERS, SLOTS, width), BF16)
    dma, dma_groups = pltpu.SemaphoreType.DMA, pltpu.SemaphoreType.DMA((GROUPS,))
    return pl.pallas_call(
        layer_kernel,
        out_shape=jax.ShapeDtypeStruct((tok, width), BF16),
        in_specs=[vm] * 9 + [hbm] * 7,
        out_specs=vm,
        scratch_shapes=[pltpu.VMEM(w.shape, w.dtype) for w in weights]
        + [boxes] * 4
        + [pltpu.VMEM((tok, width), F32), pltpu.VMEM((tok, width), BF16)]
        + [pltpu.VMEM((16, 192, 128), BF16)] * 2
        + [pltpu.VMEM((length, 128), BF16)] * 3
        + [pltpu.VMEM((256, length), F32)]
        + [pltpu.VMEM((16, 64, 128), BF16)] * 2
        + [pltpu.VMEM((tok, 1024), BF16)]
        + [pltpu.VMEM((PEERS, PEERS), F32)] * 2
        + [dma((7,)), pltpu.SemaphoreType.REGULAR]
        + [dma_groups] * 4
        + [dma] * 4,
        compiler_params=pltpu.CompilerParams(
            collective_id=1, has_side_effects=True, vmem_limit_bytes=60 * 2**20
        ),
        name="layer",
    )(q, k, v, gates, ids, rw, residual, mix_gain[None], ffn_gain[None], *weights)


def shards(
    residual_in,
    query_rows,
    key_rows,
    value_rows,
    gate_sums,
    out_weight,
    mix_gain,
    ffn_gain,
    expert_ids,
    route_weights,
    expert_gate,
    expert_up,
    expert_down,
    shared_gate,
    shared_up,
    shared_down,
):
    return layer(
        query_rows[0], key_rows[0], value_rows[0], gate_sums[0], expert_ids[0].T, route_weights[0].T,
        residual_in[0], mix_gain, ffn_gain, out_weight,
        shared_gate, shared_up, shared_down, expert_gate[0], expert_up[0], expert_down[0],
    )[None]


def solution(mesh):
    return jax.shard_map(
        shards,
        mesh=mesh,
        in_specs=(
            P("dp", "sp", None),
            P("dp", "sp", None),
            P("dp", "sp", None),
            P("dp", "sp", None),
            P("dp", "sp", None),
            P(),
            P(),
            P(),
            P("dp", "sp", None),
            P("dp", "sp", None),
            P(("sp", "dp"), None, None),
            P(("sp", "dp"), None, None),
            P(("sp", "dp"), None, None),
            P(),
            P(),
            P(),
        ),
        out_specs=P("dp", "sp", None),
        check_vma=False,
    )
```

time: 189 us -> 135 us (0.71)
  the two profiles are of different devices: /device:TPU:2 before, /device:TPU:1 now
where the time goes in v2:
time: 135 us
  Pallas kernels  133 us (99%)
  local copies, waits for them, and re-layouts  1.88 us (1%)
    pallas_call x1, Pallas kernels, layer(): pl.pallas_call(layer_kernel, out_shape=jax.ShapeDtypeStruct((tok, width),...  133 us

profile of v2, /device:TPU:1, one launch (start us, length us, event | category | flops | bytes accessed | tf_op | source)
XLA Modules:
  0.0 134.8 jit_solution(1089958954904437929)
XLA Ops:
  0.0 132.9 %layer.1 = bf16[128,2048]{1,0:T(8,128)(2,1)} custom-call(bf16[128,1024]{1,0:T(8,128)(2,1)} %bitcast.22, bf16[128,1024]{1,0:T(8,128)(2,1)} %bitcast.23, bf16[128,1024]{1,0:T(8,128)(2,1)} %bitcast.24, f32[1,2048]{1,0:T(1,128)} %bitcast.25, s32[4,128]{1,0:T(4,128)} %bitcast.28, f32[4,128]{1,0:T(4,128)} %bitcast.29, bf16[128,2048]{1,0:T(8,128)(2,1)} %bitcast.21, ...), custom_call_target="tpu_custom_call" | custom-call | tf_op jit(solution)/shard_map/layer/pallas_call | solution.py:330
  132.9 1.9 %copy.18 = bf16[1,128,2048]{2,1,0:T(8,128)(2,1)} copy(bf16[1,128,2048]{2,1,0:T(8,128)(2,1)} %bitcast.17) | data formatting | bytes 1048576

commit v3 on v2

v3 whole, which is shorter than its diff:
```python
import jax
import jax.numpy as jnp
from jax import lax
from jax.experimental import pallas as pl
from jax.experimental.pallas import tpu as pltpu
from jax.sharding import PartitionSpec as P

HEAD_DIM = 64
MESH = pl.DeviceIdType.MESH
PEERS = 128
SLOTS = 8
GROUPS = 4
PER = PEERS // GROUPS
CUTS = (slice(0, 768), slice(768, 1408), slice(1408, 2048))
F32 = jnp.float32
BF16 = jnp.bfloat16


class Torus:
    def __init__(self):
        sp, dp = lax.axis_index("sp"), lax.axis_index("dp")
        self.z, self.x, self.y, self.c = sp // 4, sp % 4, dp // 2, dp % 2
        zs = [(self.z + d) % 4 for d in range(4)]
        self.xs = [(self.x + d) % 4 for d in range(4)]
        self.ys = [(self.y + d) % 4 for d in range(4)]
        cs = [self.c, 1 - self.c]
        self.sp = [[zs[dz] * 4 + self.xs[dx] for dx in range(4)] for dz in range(4)]
        self.dp = [[self.ys[dy] * 2 + cs[dc] for dc in range(2)] for dy in range(4)]

    def at(self, dz, dx, dy, dc):
        return self.sp[dz % 4][dx % 4], self.dp[dy % 4][dc]

    def along(self, axis, d):
        return self.at(*[d if a == axis else 0 for a in range(3)], 0)

    def back(self, dz, dx, dy, dc):
        return self.sp[-dz % 4][-dx % 4], self.ys[-dy % 4] * 2 + (self.c + dc) % 2


def lane_of(axis, d, dc, a, b):
    place = [a, b]
    place.insert(axis, d)
    if isinstance(place[0], int):
        place[0] = swapped(place[0])
    return (dc, *place)


def swapped(i):
    return i % 2 * 2 + i // 2


def dot(a, b):
    return jnp.dot(a, b, preferred_element_type=F32)


def swap_matrix():
    r = lax.broadcasted_iota(jnp.int32, (256, 256), 0)
    c = lax.broadcasted_iota(jnp.int32, (256, 256), 1)
    from_row = jnp.where((c >= 64) & (c < 128), c + 64, jnp.where((c >= 128) & (c < 192), c - 64, c))
    return jnp.where(r == from_row, 1.0, 0.0).astype(BF16)


def lifted(pairs):
    r = lax.broadcasted_iota(jnp.int32, (128, 256), 0)
    c = lax.broadcasted_iota(jnp.int32, (128, 256), 1)
    out = jnp.zeros((128, 256), F32)
    for row, col, scale in pairs:
        out = jnp.where((c >= col) & (c < col + 64) & (r - row == c - col), scale, out)
    return out.astype(BF16)


def layer_kernel(
    q_ref, k_ref, v_ref, gate_ref, info_ref, res_ref, mixg_ref, ffng_ref,
    wo_any, sg_any, su_any, sd_any, eg_any, eu_any, ed_any,
    o_ref,
    wo, sg, su, sd, eg, eu, ed, outgoing, arrived, result, received, acc, normed,
    qkv_out, qkv_in, q_all, k_all, v_all, scores, att_out, heads_in, heads, info, pack_code, pack_weight, ag_z, ag_x, ag_y,
    send_z, send_x, send_y, get_z, get_x, get_y,
    wsem, ready, out_s, out_r, ret_s, ret_r, qkv_s, qkv_r, att_s, att_r, info_s, info_r, ag_s, ag_r, part_s, part_r,
):
    loads = [
        pltpu.make_async_copy(src, dst, wsem.at[i])
        for i, (src, dst) in enumerate(
            [(wo_any, wo), (sg_any, sg), (su_any, su), (sd_any, sd), (eg_any, eg), (eu_any, eu), (ed_any, ed)]
        )
    ]
    me = lax.axis_index("sp")
    barrier = pltpu.get_barrier_semaphore()

    torus = Torus()
    dp = lax.axis_index("dp")
    row = [torus.sp[k // 4][k % 4] for k in range(1, 16)]
    column = [torus.dp[k // 2][k % 2] for k in range(1, 8)]
    for to in row:
        pl.semaphore_signal(barrier, inc=1, device_id=(to, dp), device_id_type=MESH)
    for to in column:
        pl.semaphore_signal(barrier, inc=1, device_id=(me, to), device_id_type=MESH)
    for c in loads:
        c.start()

    swap = swap_matrix()
    for p in range(8):
        cols = slice(p * 128, (p + 1) * 128)
        qk = dot(jnp.concatenate([q_ref[:, cols], k_ref[:, cols]], axis=1), swap).astype(BF16)
        vv = dot(jnp.concatenate([v_ref[:64, cols], v_ref[64:, cols]], axis=1), swap).astype(BF16)
        for side in range(2):
            part = slice(side * 128, (side + 1) * 128)
            qkv_out[2 * p + side, :128, :] = qk[:, part]
            qkv_out[2 * p + side, 128:, :] = vv[:, part]
    qkv_in[me] = qkv_out[me]

    pl.semaphore_wait(barrier, 22)

    for to in row:
        pltpu.make_async_remote_copy(
            src_ref=qkv_out.at[to], dst_ref=qkv_in.at[me], send_sem=qkv_s, recv_sem=qkv_r,
            device_id=(to, dp), device_id_type=MESH,
        ).start()

    def info_copy(axis, d):
        return pltpu.make_async_remote_copy(
            src_ref=info_ref, dst_ref=info.at[axis * 3 + d - 1], send_sem=info_s, recv_sem=info_r,
            device_id=torus.along(axis, d), device_id_type=MESH,
        )

    for axis in range(3):
        for d in range(1, 4):
            info_copy(axis, d).start()

    def expert_at(dz, dx, dy, dc):
        return (((torus.z + dz) & 3) * 4 + ((torus.x + dx) & 3)) * 8 + ((torus.y + dy) & 3) * 2 + ((torus.c + dc) & 1)

    earlier = jnp.where(
        lax.broadcasted_iota(jnp.int32, (PEERS, PEERS), 0) < lax.broadcasted_iota(jnp.int32, (PEERS, PEERS), 1),
        1.0,
        0.0,
    ).astype(BF16)

    def named_in(rows, peer):
        named = jnp.zeros((peer.shape[0], PEERS), F32)
        share = jnp.zeros((peer.shape[0], PEERS), F32)
        for j in range(4):
            hit = rows[j : j + 1, :] == peer
            named = jnp.where(hit, 1.0, named)
            share = jnp.where(hit, rows[4 + j : 5 + j, :], share)
        return named, share

    def ranked(named):
        return jnp.where(named > 0.5, dot(named.astype(BF16), earlier), -1.0)

    jth = lax.broadcasted_iota(jnp.int32, (PER, 1), 0)
    jc, ja, jb = jth >> 4, (jth >> 2) & 3, jth & 3
    js = (ja & 1) * 2 + (ja >> 1)
    planes = [expert_at(0, ja, jb, jc), expert_at(js, 0, jb, jc), expert_at(js, jb, 0, jc)]
    planes = [p.astype(F32) for p in planes]
    pltpu.make_async_copy(info, info, info_r).wait()
    for axis in range(3):
        parts = [named_in(info_ref[...], planes[axis])]
        for d in range(1, 4):
            parts.append(named_in(info[axis * 3 + d - 1], planes[axis]))
        pack_code[axis] = ranked(jnp.concatenate([p[0] for p in parts], axis=0))
        pack_weight[axis] = jnp.concatenate([p[1] for p in parts], axis=0)

    pltpu.make_async_copy(qkv_in.at[pl.ds(0, 15)], qkv_in.at[pl.ds(0, 15)], qkv_r).wait()

    split_qk = lifted([(0, 0, HEAD_DIM**-0.5), (64, 128, 1.0)])
    split_v = lifted([(0, 0, 1.0), (0, 64, 1.0), (64, 128, 1.0), (64, 192, 1.0)])
    for j in range(16):
        rows = slice(j * 128, (j + 1) * 128)
        qk = dot(qkv_in[j, :128, :], split_qk).astype(BF16)
        vv = dot(qkv_in[j, 128:, :], split_v).astype(BF16)
        q_all[rows, :] = qk[:, :128]
        k_all[rows, :] = qk[:, 128:]
        v_all[j * 128 : j * 128 + 64, :] = vv[:, :128]
        v_all[j * 128 + 64 : (j + 1) * 128, :] = vv[:, 128:]

    left = lax.broadcasted_iota(jnp.int32, (64, 128), 1) < 64
    ahead = lax.broadcasted_iota(jnp.int32, (256, 256), 1) - lax.broadcasted_iota(jnp.int32, (256, 256), 0)

    def att_copy(b):
        return pltpu.make_async_remote_copy(
            src_ref=att_out.at[b], dst_ref=heads_in.at[me], send_sem=att_s, recv_sem=att_r,
            device_id=(b, dp), device_id_type=MESH,
        )

    def attend(step, _):
        turn = (me // 2 + step) % 8
        q = q_all[pl.ds(pl.multiple_of(turn * 256, 256), 256), :]
        for group in range(4):

            @pl.when(turn // 2 == group)
            def _():
                last = group * 512
                parts = [slice(c, c + 256) for c in range(0, last + 512, 256)]
                base = gate_ref[:, last : last + 1]
                top = None
                for part in parts:
                    s = lax.dot_general(
                        q, k_all[part, :], (((1,), (1,)), ((), ())), preferred_element_type=F32
                    ) + (base - gate_ref[:, part])
                    if part.start >= last:
                        s = jnp.where(ahead <= (turn % 2) * 256 - (part.start - last), s, -jnp.inf)
                    scores[:, part] = s
                    peak = jnp.maximum(s[:, :128], s[:, 128:])
                    top = peak if top is None else jnp.maximum(top, peak)
                top = jnp.max(top, axis=1, keepdims=True)
                total = None
                for part in parts:
                    e = jnp.exp(scores[:, part] - top)
                    scores[:, part] = e
                    both = e[:, :128] + e[:, 128:]
                    total = both if total is None else total + both
                inverse = 1.0 / jnp.sum(total, axis=1, keepdims=True)
                o = None
                for part in parts:
                    piece = dot((scores[:, part] * inverse).astype(BF16), v_all[part, :])
                    o = piece if o is None else o + piece
                o = o.astype(BF16)
                att_out[2 * turn] = jnp.where(left, o[:64], o[64:128])
                att_out[2 * turn + 1] = jnp.where(left, o[128:192], o[192:])

        for half in range(2):
            b = 2 * turn + half

            @pl.when(b != me)
            def _():
                att_copy(b).start()

            @pl.when(b == me)
            def _():
                heads_in[me] = att_out[me]

        return 0

    lax.fori_loop(0, 8, attend, 0)
    pltpu.make_async_copy(heads_in.at[pl.ds(0, 15)], heads_in.at[pl.ds(0, 15)], att_r).wait()
    for to in column:
        pl.semaphore_signal(ready, inc=1, device_id=(me, to), device_id_type=MESH)
    for p in range(8):
        two = dot(jnp.concatenate([heads_in[2 * p], heads_in[2 * p + 1]], axis=1), swap).astype(BF16)
        heads[:64, p * 128 : (p + 1) * 128] = two[:, :128]
        heads[64:, p * 128 : (p + 1) * 128] = two[:, 128:]

    loads[0].wait()
    projected = dot(heads[...], wo[...])
    mixed = res_ref[...].astype(F32) + mixg_ref[...] * projected * lax.rsqrt(
        jnp.mean(projected * projected, axis=1, keepdims=True) + 1e-06
    )
    acc[...] = mixed
    normed[...] = (
        ffng_ref[...] * mixed * lax.rsqrt(jnp.mean(mixed * mixed, axis=1, keepdims=True) + 1e-06)
    ).astype(BF16)
    pl.semaphore_wait(ready, 7)

    def slots_of(ranks, values):
        r = lax.broadcasted_iota(jnp.int32, (PER, SLOTS, PEERS), 1).astype(F32)
        return jnp.where(ranks[:, None, :] == r, values, 0.0).reshape(PER * SLOTS, PEERS)

    gathered = (ag_z, ag_x, ag_y)
    for axis in range(3):
        for d in range(1, 4):
            pltpu.make_async_remote_copy(
                src_ref=normed.at[:, CUTS[axis]], dst_ref=gathered[axis].at[d - 1], send_sem=ag_s.at[axis], recv_sem=ag_r.at[axis],
                device_id=torus.along(axis, d), device_id_type=MESH,
            ).start()

    def pack(axis, d):
        cut = CUTS[axis]
        source = normed[:, cut] if d == 0 else gathered[axis][d - 1]
        place = slots_of(pack_code[axis, d * PER : (d + 1) * PER, :], 1.0).astype(BF16)
        rows = dot(place, source)
        box = lane_of(axis, d, slice(None), slice(None), slice(None))
        outgoing[(*box, slice(None), cut)] = rows.reshape(2, 4, 4, SLOTS, rows.shape[1]).astype(BF16)

    def send_planes(d, axes, cores):
        for dc in cores:
            for m in range(16):
                for axis in axes:
                    a, b = m % 4, (m // 4 + m) % 4
                    if axis == 1:
                        a, b = b, a
                    box = (*lane_of(axis, d, dc, a, b), slice(None), CUTS[axis])
                    if (dc, a, b) == (0, 0, 0):
                        arrived[box] = outgoing[box]
                        continue
                    way = [a, b]
                    way.insert(axis, 0)
                    pltpu.make_async_remote_copy(
                        src_ref=outgoing.at[box], dst_ref=arrived.at[box],
                        send_sem=out_s.at[dc], recv_sem=out_r.at[dc],
                        device_id=torus.at(*way, dc), device_id_type=MESH,
                    ).start()

    for axis in range(3):
        pack(axis, 0)
    send_planes(0, range(3), (0, 1))
    for axis in range(3):
        pltpu.make_async_copy(gathered[axis], gathered[axis], ag_r.at[axis]).wait()
        for d in range(1, 4):
            pack(axis, d)
    send_planes(slice(1, 4), range(3), (0, 1))

    def taken(ref, sem, *boxes):
        for box in boxes:
            part = ref.at[box]
            pltpu.make_async_copy(part, part, sem).wait()

    def wait_planes(ref, sem, dc):
        @pl.when(dc == 0)
        def _():
            taken(ref, sem.at[0], (0, *[slice(None)] * 4, slice(0, 1920)))

        @pl.when(dc == 1)
        def _():
            taken(ref, sem.at[1], (1,))

    def wait_back(ref, sem, dc, own):
        whole, most = slice(None), slice(0, 1920)
        if dc == 0:
            box = (0, 0, whole, whole, whole, most) if own else (0, pl.ds(0, 3), whole, whole, whole, most)
        else:
            box = (1, 3) if own else (1, pl.ds(0, 3))
        taken(ref, sem.at[dc * 2 + own], box)

    def send_back(dc):
        for own, d in enumerate([slice(1, 4), 0]):
            for m in range(16):
                for axis in range(3):
                    a, b = m % 4, (m // 4 + m) % 4
                    if axis == 1:
                        a, b = b, a
                    box = (*lane_of(axis, d, dc, a, b), slice(None), CUTS[axis])
                    way = [a, b]
                    way.insert(axis, 0)

                    def remote():
                        pltpu.make_async_remote_copy(
                            src_ref=result.at[box], dst_ref=received.at[box],
                            send_sem=ret_s.at[dc * 2 + own], recv_sem=ret_r.at[dc * 2 + own],
                            device_id=torus.back(*way, dc), device_id_type=MESH,
                        ).start()

                    if (a, b) == (0, 0):

                        @pl.when(dc == 0)
                        def _():
                            received[box] = result[box]

                        pl.when(dc > 0)(remote)
                    else:
                        remote()

    def combined(axis, d):
        box = lane_of(axis, d, slice(None), slice(None), slice(None))
        rows = received[(*box, slice(None), CUTS[axis])]
        rows = rows.astype(F32).reshape(PER * SLOTS, rows.shape[4]).astype(BF16)
        part = slice(d * PER, (d + 1) * PER)
        w = slots_of(pack_code[axis, part, :], pack_weight[axis, part, :][:, None, :])
        hi = w.astype(BF16)
        lo = (w - hi.astype(F32)).astype(BF16)
        dims = (((0,), (0,)), ((), ()))
        return lax.dot_general(hi, rows, dims, preferred_element_type=F32) + lax.dot_general(
            lo, rows, dims, preferred_element_type=F32
        )

    for c in loads[1:4]:
        c.wait()
    gate = dot(normed[...], sg[...])
    up = dot(normed[...], su[...])
    hidden = (gate / (1.0 + jnp.exp(-gate)) * up).astype(BF16)
    acc[...] += dot(hidden, sd[...])
    for c in loads[4:]:
        c.wait()

    def expert(dc, h):
        here = (dc, pl.ds(h * 2, 2))
        rows = arrived[here].astype(F32).reshape(PER * SLOTS, arrived.shape[5]).astype(BF16)
        g = dot(rows, eg[...])
        u = dot(rows, eu[...])
        hid = (g / (1.0 + jnp.exp(-g)) * u).astype(BF16)
        y = dot(hid, ed[...])
        result[here] = y.reshape(2, 4, 4, SLOTS, y.shape[1]).astype(BF16)
        return dc

    def experts(dc, _):
        wait_planes(arrived, out_r, dc)
        lax.fori_loop(0, 2, lambda h, core: expert(core, h), dc)
        send_back(dc)
        return 0

    lax.fori_loop(0, 2, experts, 0)

    sends, gets = (send_z, send_x, send_y), (get_z, get_x, get_y)
    wait_back(received, ret_r, 0, 0)
    wait_back(received, ret_r, 0, 1)
    wait_back(received, ret_r, 1, 0)
    for axis in range(3):
        for d in range(1, 4):
            sends[axis][d - 1] = combined(axis, d).astype(BF16)
            pltpu.make_async_remote_copy(
                src_ref=sends[axis].at[d - 1], dst_ref=gets[axis].at[d - 1],
                send_sem=part_s.at[axis], recv_sem=part_r.at[axis],
                device_id=torus.along(axis, -d), device_id_type=MESH,
            ).start()
    wait_back(received, ret_r, 1, 1)
    for axis in range(3):
        acc[:, CUTS[axis]] += combined(axis, 0)
    for axis in range(3):
        pltpu.make_async_copy(gets[axis], gets[axis], part_r.at[axis]).wait()
        add = gets[axis][0].astype(F32) + gets[axis][1].astype(F32) + gets[axis][2].astype(F32)
        acc[:, CUTS[axis]] += add
    o_ref[...] = acc[...].astype(BF16)

    pltpu.make_async_copy(qkv_out.at[pl.ds(0, 15)], qkv_out.at[pl.ds(0, 15)], qkv_s).wait()
    pltpu.make_async_copy(att_out.at[pl.ds(0, 15)], att_out.at[pl.ds(0, 15)], att_s).wait()

    pltpu.make_async_copy(info, info, info_s).wait()
    for axis in range(3):
        pltpu.make_async_copy(gathered[axis], gathered[axis], ag_s.at[axis]).wait()
    for dc in range(2):
        wait_planes(outgoing, out_s, dc)

    for dc in range(2):
        for own in range(2):
            wait_back(result, ret_s, dc, own)
    for axis in range(3):
        pltpu.make_async_copy(sends[axis], sends[axis], part_s.at[axis]).wait()


def layer(q, k, v, gates, info, residual, mix_gain, ffn_gain, *weights):
    tok, width = residual.shape
    length = gates.shape[1]
    vm, hbm = pl.BlockSpec(memory_space=pltpu.VMEM), pl.BlockSpec(memory_space=pl.ANY)
    boxes = pltpu.VMEM((2, 4, 4, 4, SLOTS, width), BF16)
    dma, dma_groups = pltpu.SemaphoreType.DMA, pltpu.SemaphoreType.DMA((GROUPS,))
    return pl.pallas_call(
        layer_kernel,
        out_shape=jax.ShapeDtypeStruct((tok, width), BF16),
        in_specs=[vm] * 8 + [hbm] * 7,
        out_specs=vm,
        scratch_shapes=[pltpu.VMEM(w.shape, w.dtype) for w in weights]
        + [boxes] * 4
        + [pltpu.VMEM((tok, width), F32), pltpu.VMEM((tok, width), BF16)]
        + [pltpu.VMEM((16, 192, 128), BF16)] * 2
        + [pltpu.VMEM((length, 128), BF16)] * 3
        + [pltpu.VMEM((256, length), F32)]
        + [pltpu.VMEM((16, 64, 128), BF16)] * 2
        + [pltpu.VMEM((tok, 1024), BF16)]
        + [pltpu.VMEM((9, 8, tok), F32)]
        + [pltpu.VMEM((3, PEERS, PEERS), F32)] * 2
        + [pltpu.VMEM((3, tok, cut.stop - cut.start), BF16) for cut in CUTS] * 3
        + [dma((7,)), pltpu.SemaphoreType.REGULAR]
        + [pltpu.SemaphoreType.DMA((2,))] * 2
        + [dma_groups] * 2
        + [dma] * 6
        + [dma((3,))] * 4,
        compiler_params=pltpu.CompilerParams(
            collective_id=1, has_side_effects=True, vmem_limit_bytes=60 * 2**20
        ),
        name="layer",
    )(q, k, v, gates, info, residual, mix_gain[None], ffn_gain[None], *weights)


def shards(
    residual_in,
    query_rows,
    key_rows,
    value_rows,
    gate_sums,
    out_weight,
    mix_gain,
    ffn_gain,
    expert_ids,
    route_weights,
    expert_gate,
    expert_up,
    expert_down,
    shared_gate,
    shared_up,
    shared_down,
):
    info = jnp.concatenate([expert_ids[0].astype(F32), route_weights[0]], axis=1).T
    return layer(
        query_rows[0], key_rows[0], value_rows[0], gate_sums[0], info,
        residual_in[0], mix_gain, ffn_gain, out_weight,
        shared_gate, shared_up, shared_down, expert_gate[0], expert_up[0], expert_down[0],
    )[None]


def solution(mesh):
    return jax.shard_map(
        shards,
        mesh=mesh,
        in_specs=(
            P("dp", "sp", None),
            P("dp", "sp", None),
            P("dp", "sp", None),
            P("dp", "sp", None),
            P("dp", "sp", None),
            P(),
            P(),
            P(),
            P("dp", "sp", None),
            P("dp", "sp", None),
            P(("sp", "dp"), None, None),
            P(("sp", "dp"), None, None),
            P(("sp", "dp"), None, None),
            P(),
            P(),
            P(),
        ),
        out_specs=P("dp", "sp", None),
        check_vma=False,
    )
```

time: 135 us -> 122 us (0.904)
  Pallas kernels: 133 us -> 118 us
  other arithmetic: 0 us -> 1.96 us
    pallas_call x1, Pallas kernels: 133 us -> 118 us  [layer(): pl.pallas_call(layer_kernel, out_shape=jax.ShapeDtypeStruct((tok, width),...]
where the time goes in v3:
time: 122 us
  Pallas kernels  118 us (97%)
  other arithmetic  1.96 us (2%)
  local copies, waits for them, and re-layouts  1.88 us (2%)
    pallas_call x1, Pallas kernels, layer(): pl.pallas_call(layer_kernel, out_shape=jax.ShapeDtypeStruct((tok, width),...  118 us

profile of v3, /device:TPU:1, one launch (start us, length us, event | category | flops | bytes accessed | tf_op | source)
XLA Modules:
  0.0 121.6 jit_solution(7740542854477945271)
XLA Ops:
  0.0 0.7 convert_bitcast_fusion
  0.7 1.3 %maximum_bitcast_fusion.info_ref = f32[8,128]{1,0:T(8,128)} fusion(f32[128,4]{0,1:T(4,128)} %bitcast.27, f32[128,4]{0,1:T(4,128)S(1)} %convert_bitcast_fusion), kind=kLoop, calls=%fused_computation | loop fusion | flops 1024 | bytes 8192 | tf_op jit(solution)/shard_map/transpose | solution.py:482
  2.0 117.8 %layer.1 = bf16[128,2048]{1,0:T(8,128)(2,1)} custom-call(bf16[128,1024]{1,0:T(8,128)(2,1)} %bitcast.21, bf16[128,1024]{1,0:T(8,128)(2,1)} %bitcast.22, bf16[128,1024]{1,0:T(8,128)(2,1)} %bitcast.23, f32[1,2048]{1,0:T(1,128)} %bitcast.24, f32[8,128]{1,0:T(8,128)} %maximum_bitcast_fusion.info_ref, bf16[128,2048]{1,0:T(8,128)(2,1)} %bitcast.20, ...), custom_call_target="tpu_custom_call" | custom-call | tf_op jit(solution)/shard_map/layer/pallas_call | solution.py:436
  119.7 1.9 %copy.18 = bf16[1,128,2048]{2,1,0:T(8,128)(2,1)} copy(bf16[1,128,2048]{2,1,0:T(8,128)(2,1)} %bitcast.16) | data formatting | bytes 1048576

commit v4 on v3

--- a/solution.py
+++ b/solution.py
@@ -89,7 +89,7 @@
 
     torus = Torus()
     dp = lax.axis_index("dp")
-    row = [torus.sp[k // 4][k % 4] for k in range(1, 16)]
+    row = [torus.sp[k % 4][(k // 4 + k) % 4] for k in range(1, 16)]
     column = [torus.dp[k // 2][k % 2] for k in range(1, 8)]
     for to in row:
         pl.semaphore_signal(barrier, inc=1, device_id=(to, dp), device_id_type=MESH)
@@ -257,8 +257,8 @@
         return jnp.where(ranks[:, None, :] == r, values, 0.0).reshape(PER * SLOTS, PEERS)
 
     gathered = (ag_z, ag_x, ag_y)
-    for axis in range(3):
-        for d in range(1, 4):
+    for d in (2, 1, 3):
+        for axis in range(3):
             pltpu.make_async_remote_copy(
                 src_ref=normed.at[:, CUTS[axis]], dst_ref=gathered[axis].at[d - 1], send_sem=ag_s.at[axis], recv_sem=ag_r.at[axis],
                 device_id=torus.along(axis, d), device_id_type=MESH,
@@ -394,8 +394,8 @@
     wait_back(received, ret_r, 0, 0)
     wait_back(received, ret_r, 0, 1)
     wait_back(received, ret_r, 1, 0)
-    for axis in range(3):
-        for d in range(1, 4):
+    for d in (2, 1, 3):
+        for axis in range(3):
             sends[axis][d - 1] = combined(axis, d).astype(BF16)
             pltpu.make_async_remote_copy(
                 src_ref=sends[axis].at[d - 1], dst_ref=gets[axis].at[d - 1],

time: 122 us -> 121 us (level)
  no operation moved by 1% of the time
where the time goes in v4:
time: 121 us; the launch traced here: 120 us
  Pallas kernels  117 us (97%)
  other arithmetic  1.96 us (2%)
  local copies, waits for them, and re-layouts  1.88 us (2%)
    pallas_call x1, Pallas kernels, layer(): pl.pallas_call(layer_kernel, out_shape=jax.ShapeDtypeStruct((tok, width),...  117 us

profile of v4, /device:TPU:1, one launch (start us, length us, event | category | flops | bytes accessed | tf_op | source)
XLA Modules:
  0.0 120.4 jit_solution(16794084887746386122)
XLA Ops:
  0.0 0.7 convert_bitcast_fusion
  0.7 1.3 %maximum_bitcast_fusion.info_ref = f32[8,128]{1,0:T(8,128)} fusion(f32[128,4]{0,1:T(4,128)} %bitcast.27, f32[128,4]{0,1:T(4,128)S(1)} %convert_bitcast_fusion), kind=kLoop, calls=%fused_computation | loop fusion | flops 1024 | bytes 8192 | tf_op jit(solution)/shard_map/transpose | solution.py:482
  2.0 116.6 %layer.1 = bf16[128,2048]{1,0:T(8,128)(2,1)} custom-call(bf16[128,1024]{1,0:T(8,128)(2,1)} %bitcast.21, bf16[128,1024]{1,0:T(8,128)(2,1)} %bitcast.22, bf16[128,1024]{1,0:T(8,128)(2,1)} %bitcast.23, f32[1,2048]{1,0:T(1,128)} %bitcast.24, f32[8,128]{1,0:T(8,128)} %maximum_bitcast_fusion.info_ref, bf16[128,2048]{1,0:T(8,128)(2,1)} %bitcast.20, ...), custom_call_target="tpu_custom_call" | custom-call | tf_op jit(solution)/shard_map/layer/pallas_call | solution.py:436
  118.6 1.9 %copy.18 = bf16[1,128,2048]{2,1,0:T(8,128)(2,1)} copy(bf16[1,128,2048]{2,1,0:T(8,128)(2,1)} %bitcast.16) | data formatting | bytes 1048576
